TPU v7x, 32 devices: a whole 2x2x4 slice. The times are simulated.
32 devices in a mesh: ep: 8 (over z, core), tp: 4 (over y, x).
Axes of the slice: x: 2, y: 2, z: 4, core: 2. Of those that a mesh axis runs over, the one named last changes fastest.
Arguments:
- tokens: bfloat16 [256, 4096], P('ep'), may hold values from -6 to 6
- recur_state: float32 [256, 4096], P('ep', 'tp'), may hold values from -6 to 6
- conv_state: bfloat16 [256, 3, 4096], P('ep', None, 'tp'), may hold values from -6 to 6
- mix_gain: float32 [4096], replicated, may hold values from 0.1 to 1.9
- in_weight: bfloat16 [4096, 4096], P('ep', 'tp'), may hold values from -0.09375 to 0.09375
- gate_weight: bfloat16 [4096, 4096], P('ep', 'tp'), may hold values from -0.09375 to 0.09375
- conv_taps: float32 [4, 4096], P(None, 'tp'), may hold values from -3 to 3
- recur_gate_blocks: bfloat16 [64, 64, 64], P('tp'), may hold values from -0.75 to 0.75
- input_gate_blocks: bfloat16 [64, 64, 64], P('tp'), may hold values from -0.75 to 0.75
- decay_rate: float32 [4096], P('tp'), may hold values from 0.01 to 0.4
- out_weight: bfloat16 [4096, 4096], P('tp', 'ep'), may hold values from -0.09375 to 0.09375
- ffn_gain: float32 [4096], replicated, may hold values from 0.1 to 1.9
- router_weight: bfloat16 [4096, 8], replicated, may hold values from -0.09375 to 0.09375
- routes: int32 [256, 2], P('ep'), may hold values from 0 to 7, as said below
- expert_gate: bfloat16 [8, 4096, 2048], P('ep', None, 'tp'), may hold values from -0.09375 to 0.09375
- expert_up: bfloat16 [8, 4096, 2048], P('ep', None, 'tp'), may hold values from -0.09375 to 0.09375
- expert_down: bfloat16 [8, 2048, 4096], P('ep', 'tp'), may hold values from -0.125 to 0.125
- dense_gate: bfloat16 [4096, 2048], P('ep', 'tp'), may hold values from -0.09375 to 0.09375
- dense_up: bfloat16 [4096, 2048], P('ep', 'tp'), may hold values from -0.09375 to 0.09375
- dense_down: bfloat16 [2048, 4096], P('tp', 'ep'), may hold values from -0.125 to 0.125
- branch_gate: bfloat16 [4096], replicated, may hold values from -0.09375 to 0.09375
Outputs:
- layer_out: bfloat16 [256, 4096], P('ep')
- new_state: float32 [256, 4096], P('ep', 'tp')
- new_conv_state: bfloat16 [256, 3, 4096], P('ep', None, 'tp')
Inputs may be any that keep to these rules, and one draw needn't show every extreme that they name: `routes`: A row names two different experts of one group: both have the same e // 4. In the rows of one index of ep no expert is named more than 16 times, and in every draw some expert is named exactly 16 times by the rows of every index of ep.
All inputs are finite; a program needn't handle non-finite values.
Results may differ from a plain program's by a relative error of at most 0.023.
Values may be sent and summed in bfloat16 or wider, within the bound.
A program may use at most 64 MiB of HBM per device.

v0:
```python
import jax
import jax.numpy as jnp
from jax import lax
from jax.sharding import PartitionSpec as P

TOP_K = 2
epsilon = 1e-06
decay_scale = 8.0


def rms_scale(rows, gain):
    values = rows.astype(jnp.float32)
    inverse = lax.rsqrt(jnp.mean(values * values, axis=-1, keepdims=True) + epsilon)
    return (values * inverse * gain).astype(jnp.bfloat16)


def on_device(
    tokens,
    recur_state,
    conv_state,
    mix_gain,
    in_weight,
    gate_weight,
    conv_taps,
    recur_gate_blocks,
    input_gate_blocks,
    decay_rate,
    out_weight,
    ffn_gain,
    router_weight,
    routes,
    expert_gate,
    expert_up,
    expert_down,
    dense_gate,
    dense_up,
    dense_down,
    branch_gate,
):
    batch_rows, width = tokens.shape
    channels = in_weight.shape[1]
    normed = rms_scale(tokens, mix_gain)
    arrived = lax.all_to_all(normed, "ep", split_axis=1, concat_axis=0, tiled=True)
    joined = jnp.concatenate([in_weight, gate_weight], axis=1)
    summed = lax.psum_scatter(
        jnp.dot(arrived, joined, preferred_element_type=jnp.float32).astype(jnp.bfloat16),
        "ep",
        scatter_dimension=0,
        tiled=True,
    ).astype(jnp.float32)
    x_sum, gate_sum = (summed[:, :channels], summed[:, channels:])
    x_branch = x_sum.astype(jnp.bfloat16)
    gate_branch = gate_sum.astype(jnp.bfloat16)
    window = jnp.concatenate([conv_state, x_branch[:, None, :]], axis=1)
    conv_out = jnp.sum(window.astype(jnp.float32) * conv_taps[None], axis=1).astype(jnp.bfloat16)
    new_conv_state = window[:, 1:, :]
    blocks = conv_out.reshape(batch_rows, recur_gate_blocks.shape[0], recur_gate_blocks.shape[1])
    recur_gate = jax.nn.sigmoid(
        jnp.einsum(
            "bhi,hij->bhj", blocks, recur_gate_blocks, preferred_element_type=jnp.float32
        ).reshape(batch_rows, channels)
    )
    input_gate = jax.nn.sigmoid(
        jnp.einsum(
            "bhi,hij->bhj", blocks, input_gate_blocks, preferred_element_type=jnp.float32
        ).reshape(batch_rows, channels)
    )
    log_decay = -decay_scale * recur_gate * decay_rate
    new_state = jnp.exp(log_decay) * recur_state + jnp.sqrt(
        -jnp.expm1(2.0 * log_decay)
    ) * input_gate * conv_out.astype(jnp.float32)
    mixer_rows = (new_state * jax.nn.gelu(gate_branch.astype(jnp.float32))).astype(jnp.bfloat16)
    mixer_part = jnp.dot(
        mixer_rows,
        lax.all_gather(out_weight, "ep", axis=1, tiled=True),
        preferred_element_type=jnp.float32,
    )
    resid = (
        tokens.astype(jnp.float32)
        + lax.psum(mixer_part.astype(jnp.bfloat16), "tp").astype(jnp.float32)
    ).astype(jnp.bfloat16)
    normed_ffn = rms_scale(resid, ffn_gain)
    router_logits = jnp.dot(normed_ffn, router_weight, preferred_element_type=jnp.float32)
    experts = router_logits.shape[1]
    expert_ids = lax.broadcasted_iota(jnp.int32, (batch_rows, TOP_K, experts), 2)
    picked = jnp.sum(
        jnp.where(routes[:, :, None] == expert_ids, router_logits[:, None, :], 0.0), axis=2
    )
    route_weight = jax.nn.sigmoid(picked - picked[:, ::-1]).astype(jnp.bfloat16)
    capacity = 2 * batch_rows * TOP_K // experts
    flat_ids = routes.reshape(batch_rows * TOP_K)
    onehot = (
        flat_ids[:, None] == lax.broadcasted_iota(jnp.int32, (batch_rows * TOP_K, experts), 1)
    ).astype(jnp.int32)
    rank = jnp.sum((jnp.cumsum(onehot, axis=0) - onehot) * onehot, axis=1)
    slot_of = (flat_ids * capacity + rank).reshape(batch_rows, TOP_K)
    slot_rows = lax.broadcasted_iota(jnp.int32, (experts * capacity, batch_rows), 0)
    slot_cols = lax.broadcasted_iota(jnp.int32, (batch_rows, experts * capacity), 1)
    dispatch = jnp.zeros((experts * capacity, batch_rows), jnp.bfloat16)
    combine = jnp.zeros((batch_rows, experts * capacity), jnp.bfloat16)
    for pick in range(TOP_K):
        dispatch = dispatch + (slot_rows == slot_of[None, :, pick]).astype(jnp.bfloat16)
        combine = combine + jnp.where(
            slot_cols == slot_of[:, pick : pick + 1],
            route_weight[:, pick : pick + 1],
            jnp.zeros((), jnp.bfloat16),
        )
    outgoing = (
        jnp.dot(dispatch, normed_ffn, preferred_element_type=jnp.float32)
        .astype(jnp.bfloat16)
        .reshape(experts, capacity, width)
    )
    gate_local = expert_gate[0]
    up_local = expert_up[0]
    down_local = expert_down[0]
    arrived_rows = lax.all_to_all(outgoing, "ep", split_axis=0, concat_axis=0, tiled=True)
    sources, items, features = arrived_rows.shape
    rows = arrived_rows.reshape(sources * items, features)
    first = jnp.dot(rows, gate_local, preferred_element_type=jnp.float32)
    second = jnp.dot(rows, up_local, preferred_element_type=jnp.float32)
    act = (jax.nn.silu(first) * second).astype(jnp.bfloat16)
    partial_value = jnp.dot(act, down_local, preferred_element_type=jnp.float32)
    total = lax.psum(partial_value.astype(jnp.bfloat16), "tp")
    returned = lax.all_to_all(
        total.reshape(sources, items, total.shape[1]), "ep", split_axis=0, concat_axis=0, tiled=True
    )
    moe = jnp.dot(
        combine,
        returned.reshape(experts * capacity, returned.shape[2]),
        preferred_element_type=jnp.float32,
    )
    dense_arrived = lax.all_to_all(normed_ffn, "ep", split_axis=1, concat_axis=0, tiled=True)
    dense_joined = jnp.concatenate([dense_gate, dense_up], axis=1)
    dense_summed = lax.psum_scatter(
        jnp.dot(dense_arrived, dense_joined, preferred_element_type=jnp.float32).astype(
            jnp.bfloat16
        ),
        "ep",
        scatter_dimension=0,
        tiled=True,
    ).astype(jnp.float32)
    dense_first = dense_summed[:, : dense_gate.shape[1]]
    dense_second = dense_summed[:, dense_gate.shape[1] :]
    dense_act = (jax.nn.silu(dense_first) * dense_second).astype(jnp.bfloat16)
    dense_part = jnp.dot(
        dense_act,
        lax.all_gather(dense_down, "ep", axis=1, tiled=True),
        preferred_element_type=jnp.float32,
    )
    branch_weight = jax.nn.sigmoid(
        jnp.dot(normed_ffn, branch_gate, preferred_element_type=jnp.float32)
    )
    dense_sum = lax.psum(dense_part.astype(jnp.bfloat16), "tp").astype(jnp.float32)
    layer_out = (resid.astype(jnp.float32) + moe + branch_weight[:, None] * dense_sum).astype(
        jnp.bfloat16
    )
    return (layer_out, new_state, new_conv_state)


def solution(mesh):
    in_specs = (
        P("ep", None),
        P("ep", "tp"),
        P("ep", None, "tp"),
        P(),
        P("ep", "tp"),
        P("ep", "tp"),
        P(None, "tp"),
        P("tp", None, None),
        P("tp", None, None),
        P("tp"),
        P("tp", "ep"),
        P(),
        P(),
        P("ep", None),
        P("ep", None, "tp"),
        P("ep", None, "tp"),
        P("ep", "tp", None),
        P("ep", "tp"),
        P("ep", "tp"),
        P("tp", "ep"),
        P(),
    )
    out_specs = (P("ep", None), P("ep", "tp"), P("ep", None, "tp"))
    return jax.shard_map(
        on_device, mesh=mesh, in_specs=in_specs, out_specs=out_specs, check_vma=False
    )
```

profile of v0, /device:TPU:0, one launch (start us, length us, event | category | flops | bytes accessed | tf_op | source)
XLA Modules:
  0.0 396.9 jit_solution(11186199223250125864)
XLA Ops:
  7.2 1.1 fusion.33
  8.4 1.1 fusion.35
  9.5 16.0 %all_to_all.48 = bf16[32,8,512]{2,0,1:T(8,128)(2,1)S(1)} all-to-all(bf16[32,8,512]{2,0,1:T(8,128)(2,1)S(1)} %bitcast.77), channel_id=1, replica_groups=mesh['ep'=8,'tp'=4] {'ep'}, dimensions={1} | all-to-all | bytes 524288 | tf_op jit(solution)/shard_map/all_to_all | solution.py:43
  25.5 3.4 convolution_convert_fusion.4
  29.8 30.9 %reduce-scatter.3.cloned.1.call-done = bf16[32,2048]{1,0:T(8,128)(2,1)} async-done(((bf16[256,2048]{1,0:T(8,128)(2,1)}), bf16[32,2048]{1,0:T(8,128)(2,1)}) %reduce-scatter.3.cloned.1.call-update) | async-done | bytes 131088 | tf_op jit(solution)/shard_map/reduce_scatter | solution.py:45
  60.7 0.9 slice_bitcast_fusion
  63.1 79.5 %all-gather.3.cloned.1.call-done = bf16[1024,4096]{1,0:T(8,128)(2,1)} async-done(((bf16[1024,512]{1,0:T(8,128)(2,1)}), bf16[1024,4096]{1,0:T(8,128)(2,1)}) %all-gather.3.cloned.1.call-update) | async-done | bytes 8388624 | tf_op jit(solution)/shard_map/all_gather | solution.py:75
  142.5 5.6 %convolution_convert_fusion.3 = bf16[32,4096]{1,0:T(8,128)(2,1)} fusion(bf16[1024,4096]{1,0:T(8,128)(2,1)} %all-gather.3.cloned.1.call-done, f32[32,1024]{1,0:T(8,128)S(1)} %multiply_add_fusion, bf16[32,2048]{1,0:T(8,128)(2,1)S(1)} %copy-done.5), kind=kOutput, calls=%fused_computation.6 | convolution fusion | flops 268926976 | bytes 8847360 | tf_op jit(solution)/shard_map/dot_general | solution.py:73
  148.2 41.6 %all-reduce.4.cloned.1.call-done = bf16[32,4096]{1,0:T(8,128)(2,1)} async-done(((bf16[32,4096]{1,0:T(8,128)(2,1)}), bf16[32,4096]{1,0:T(8,128)(2,1)}) %all-reduce.4.cloned.1.call-update) | async-done | bytes 262160 | tf_op jit(solution)/shard_map/psum | solution.py:80
  189.9 1.1 fusion.37
  191.0 1.1 fusion.39
  192.1 14.1 %all_to_all.49 = bf16[32,8,512]{2,0,1:T(8,128)(2,1)S(1)} all-to-all(bf16[32,8,512]{2,0,1:T(8,128)(2,1)S(1)} %bitcast.78), channel_id=1, replica_groups=mesh['ep'=8,'tp'=4] {'ep'}, dimensions={1} | all-to-all | bytes 524288 | tf_op jit(solution)/shard_map/all_to_all | solution.py:132
  206.2 1.3 convolution_convert_fusion.5
  208.9 1.4 convolution_convert_fusion.1
  210.3 3.6 all-to-all-start.1
  213.9 24.5 %reduce-scatter.5.cloned.1.call-done = bf16[32,1024]{1,0:T(8,128)(2,1)} async-done(((bf16[256,1024]{1,0:T(8,128)(2,1)}), bf16[32,1024]{1,0:T(8,128)(2,1)}) %reduce-scatter.5.cloned.1.call-update) | async-done | bytes 65552 | tf_op jit(solution)/shard_map/reduce_scatter | solution.py:134
  239.2 49.8 %all-gather.5.cloned.1.call-done = bf16[512,4096]{1,0:T(8,128)(2,1)} async-done(((bf16[512,512]{1,0:T(8,128)(2,1)}), bf16[512,4096]{1,0:T(8,128)(2,1)}) %all-gather.5.cloned.1.call-update) | async-done | bytes 4194320 | tf_op jit(solution)/shard_map/all_gather | solution.py:147
  289.0 3.7 convolution_convert_fusion.2
  292.7 2.9 fusion.5
  295.7 5.9 %convolution_convert_fusion = bf16[128,4096]{1,0:T(8,128)(2,1)} fusion(bf16[1,512,4096]{2,1,0:T(8,128)(2,1)} %param.37, bf16[128,4096]{1,0:T(8,128)(2,1)S(1)} %bitcast.72, bf16[1,4096,512]{2,1,0:T(8,128)(2,1)} %param.36, f32[128,512]{1,0:T(8,128)S(1)} %fusion.5), kind=kOutput, calls=%fused_computation | convolution fusion | flops 1074659328 | bytes 10747904 | tf_op jit(solution)/shard_map/dot_general | solution.py:122
  301.6 55.4 %all-reduce.6.cloned.1.call-done = (bf16[8,16,4096]{2,1,0:T(8,128)(2,1)}, bf16[32,4096]{1,0:T(8,128)(2,1)}) async-done(((bf16[8,16,4096]{2,1,0:T(8,128)(2,1)}, bf16[32,4096]{1,0:T(8,128)(2,1)}), (bf16[8,16,4096]{2,1,0:T(8,128)(2,1)}, bf16[32,4096]{1,0:T(8,128)(2,1)})) %all-reduce.6.cloned.1.call-update) | async-done | bytes 1310736 | tf_op jit(solution)/shard_map/psum | solution.py:123
  356.9 4.6 %all-to-all-start.2 = ((bf16[8,16,4096]{2,1,0:T(8,128)(2,1)}), bf16[8,16,4096]{2,1,0:T(8,128)(2,1)S(1)}, u32[]{:S(2)}, u32[]{:S(2)}) async-start(bf16[8,16,4096]{2,1,0:T(8,128)(2,1)} %get-tuple-element.3), calls=%async_computation.3 | async-start | bytes 2097152 | tf_op jit(solution)/shard_map/all_to_all | solution.py:124
  362.7 25.4 %all-to-all-done.2 = bf16[8,16,4096]{2,1,0:T(8,128)(2,1)S(1)} async-done(((bf16[8,16,4096]{2,1,0:T(8,128)(2,1)}), bf16[8,16,4096]{2,1,0:T(8,128)(2,1)S(1)}, u32[]{:S(2)}, u32[]{:S(2)}) %all-to-all-start.2) | async-done | bytes 1048608 | tf_op jit(solution)/shard_map/all_to_all | solution.py:124
  388.1 2.0 fusion.1
  (77 shorter events, 5.7 us)
Async XLA Ops:
  7.2 54.7 %copy-start = (bf16[16,64,64]{2,1,0:T(8,128)(2,1)S(1)}, bf16[16,64,64]{2,1,0:T(8,128)(2,1)}, u32[]{:S(2)}) copy-start(bf16[16,64,64]{2,1,0:T(8,128)(2,1)} %param.28) | copy-start | bytes 393220
  7.2 53.5 %reduce-scatter.3.cloned.1.call-start = ((), (), s32[]{:S(2)}) async-start(), calls=%async_computation.6 | async-start | bytes 1179648 | tf_op jit(solution)/shard_map/reduce_scatter | solution.py:45
  8.4 21.4 %copy-start.12 = (f32[1024]{0:T(1024)S(1)}, f32[1024]{0:T(1024)}, u32[]{:S(2)}) copy-start(f32[1024]{0:T(1024)} %param.30) | copy-start | bytes 12292
  9.5 52.1 %copy-start.4 = (bf16[32,3,1024]{2,0,1:T(8,128)(2,1)S(1)}, bf16[32,3,1024]{2,0,1:T(8,128)(2,1)}, u32[]{:S(2)}) copy-start(bf16[32,3,1024]{2,0,1:T(8,128)(2,1)} %param.23) | copy-start | bytes 589828
  9.5 52.1 %copy-start.9 = (f32[4,1024]{1,0:T(4,128)S(1)}, f32[4,1024]{1,0:T(4,128)}, u32[]{:S(2)}) copy-start(f32[4,1024]{1,0:T(4,128)} %param.27) | copy-start | bytes 49156
  25.5 36.8 %copy-start.15 = (bf16[16,64,64]{2,1,0:T(8,128)(2,1)S(1)}, bf16[16,64,64]{2,1,0:T(8,128)(2,1)}, u32[]{:S(2)}) copy-start(bf16[16,64,64]{2,1,0:T(8,128)(2,1)} %param.29) | copy-start | bytes 393220
  28.9 34.0 %copy-start.6 = (f32[32,1024]{1,0:T(8,128)S(1)}, f32[32,1024]{1,0:T(8,128)}, u32[]{:S(2)}) copy-start(f32[32,1024]{1,0:T(8,128)} %param.22) | copy-start | bytes 393220
  28.9 113.6 %all-gather.3.cloned.1.call-start = ((), (), s32[]{:S(2)}) async-start(), calls=%async_computation.7 | async-start | bytes 9437184 | tf_op jit(solution)/shard_map/all_gather | solution.py:75
  29.7 160.2 %all-reduce.4.cloned.1.call-start = ((), (), s32[]{:S(2)}) async-start(), calls=%async_computation.8 | async-start | bytes 524288 | tf_op jit(solution)/shard_map/psum | solution.py:80
  60.7 81.8 %copy-start.5 = (bf16[32,2048]{1,0:T(8,128)(2,1)S(1)}, bf16[32,2048]{1,0:T(8,128)(2,1)}, u32[]{:S(2)}) copy-start(bf16[32,2048]{1,0:T(8,128)(2,1)} %reduce-scatter.3.cloned.1.call-done) | copy-start | bytes 393220
  63.0 85.1 %copy-start.3 = (f32[32,1024]{1,0:T(8,128)}, f32[32,1024]{1,0:T(8,128)S(1)}, u32[]{:S(2)}) copy-start(f32[32,1024]{1,0:T(8,128)S(1)} %multiply_add_fusion) | copy-start | bytes 393220
  63.0 126.8 %copy-start.1 = (bf16[32,4096]{1,0:T(8,128)(2,1)S(1)}, bf16[32,4096]{1,0:T(8,128)(2,1)}, u32[]{:S(2)}) copy-start(bf16[32,4096]{1,0:T(8,128)(2,1)} %param.21) | copy-start | bytes 786436
  63.0 128.0 %copy-start.8 = (f32[4096]{0:T(1024)S(1)}, f32[4096]{0:T(1024)}, u32[]{:S(2)}) copy-start(f32[4096]{0:T(1024)} %param.32) | copy-start | bytes 49156
  63.1 143.2 %copy-start.13 = (bf16[512,512]{1,0:T(8,128)(2,1)S(1)}, bf16[512,512]{1,0:T(8,128)(2,1)}, u32[]{:S(2)}) copy-start(bf16[512,512]{1,0:T(8,128)(2,1)} %param.39) | copy-start | bytes 1572868
  63.1 143.2 %copy-start.14 = (bf16[512,512]{1,0:T(8,128)(2,1)S(1)}, bf16[512,512]{1,0:T(8,128)(2,1)}, u32[]{:S(2)}) copy-start(bf16[512,512]{1,0:T(8,128)(2,1)} %param.38) | copy-start | bytes 1572868
  148.2 60.0 %copy-start.10 = (s32[32,2]{0,1:T(2,128)S(1)}, s32[32,2]{0,1:T(2,128)}, u32[]{:S(2)}) copy-start(s32[32,2]{0,1:T(2,128)} %param.34) | copy-start | bytes 772
  148.2 90.2 %reduce-scatter.5.cloned.1.call-start = ((), (), s32[]{:S(2)}) async-start(), calls=%async_computation.9 | async-start | bytes 589824 | tf_op jit(solution)/shard_map/reduce_scatter | solution.py:134
  207.6 81.4 %all-gather.5.cloned.1.call-start = ((), (), s32[]{:S(2)}) async-start(), calls=%async_computation.10 | async-start | bytes 4718592 | tf_op jit(solution)/shard_map/all_gather | solution.py:147
  210.3 82.4 %all-to-all-start.1 = ((bf16[8,16,4096]{2,1,0:T(8,128)(2,1)}), bf16[8,16,4096]{2,1,0:T(8,128)(2,1)S(1)}, u32[]{:S(2)}, u32[]{:S(2)}) async-start(bf16[8,16,4096]{2,1,0:T(8,128)(2,1)} %bitcast.9), calls=%async_computation.2 | async-start | bytes 2097152 | tf_op jit(solution)/shard_map/all_to_all | solution.py:116
  213.9 143.0 %all-reduce.6.cloned.1.call-start = ((), (), s32[]{:S(2)}) async-start(), calls=%async_computation.11 | async-start | bytes 2621440 | tf_op jit(solution)/shard_map/psum | solution.py:123
  295.6 65.9 %copy-start.11 = (bf16[4096]{0:T(1024)(128)(2,1)S(1)}, bf16[4096]{0:T(1024)(128)(2,1)}, u32[]{:S(2)}) copy-start(bf16[4096]{0:T(1024)(128)(2,1)} %param.41) | copy-start | bytes 24580
  295.6 66.6 %copy-start.7 = (bf16[4096,8]{0,1:T(8,128)(2,1)S(1)}, bf16[4096,8]{0,1:T(8,128)(2,1)}, u32[]{:S(2)}) copy-start(bf16[4096,8]{0,1:T(8,128)(2,1)} %param.33) | copy-start | bytes 196612
  301.5 86.5 %copy-start.2 = (bf16[32,4096]{1,0:T(8,128)(2,1)S(1)}, bf16[32,4096]{1,0:T(8,128)(2,1)}, u32[]{:S(2)}) copy-start(bf16[32,4096]{1,0:T(8,128)(2,1)} %all-reduce.4.cloned.1.call-done) | copy-start | bytes 786436
  356.9 31.2 %all-to-all-start.2 = ((bf16[8,16,4096]{2,1,0:T(8,128)(2,1)}), bf16[8,16,4096]{2,1,0:T(8,128)(2,1)S(1)}, u32[]{:S(2)}, u32[]{:S(2)}) async-start(bf16[8,16,4096]{2,1,0:T(8,128)(2,1)} %get-tuple-element.3), calls=%async_computation.3 | async-start | bytes 2097152 | tf_op jit(solution)/shard_map/all_to_all | solution.py:124
Sparse Core Ops, SparseCore 0:
  29.1 31.6 reduce-scatter.2
  62.3 80.1 all-gather.2
  148.3 41.5 all-reduce.3
  207.7 30.6 reduce-scatter.4
  239.8 49.1 all-gather.4
  301.7 55.1 all-reduce.5
where the time goes:
time: 398 us; the launch traced here: 397 us
  waiting for transfers between devices  308 us (77%)
  blocking collectives  30.1 us (8%)
  matrix products  26.9 us (7%)
  between operations  14.4 us (4%)
  starting transfers between devices  8.4 us (2%)
  other arithmetic  6.59 us (2%)
    all_gather x1, waiting for transfers between devices, on_device(): lax.all_gather(out_weight, 'ep', axis=1, tiled=True)  79.5 us
    psum x1, waiting for transfers between devices, on_device(): total = lax.psum(partial_value.astype(jnp.bfloat16), 'tp')  55.4 us
    all_gather x1, waiting for transfers between devices, on_device(): lax.all_gather(dense_down, 'ep', axis=1, tiled=True)  49.8 us
    psum x1, waiting for transfers between devices, on_device(): lax.psum(mixer_part.astype(jnp.bfloat16), 'tp').astype(jnp.float32)  41.6 us
    reduce_scatter x1, waiting for transfers between devices, on_device(): lax.psum_scatter(jnp.dot(arrived, joined, preferred_element_type=jnp.floa...  30.9 us
    all_to_all x1, waiting for transfers between devices, on_device(): lax.all_to_all(total.reshape(sources, items, total.shape[1]), 'ep', split...  25.4 us
    reduce_scatter x1, waiting for transfers between devices, on_device(): lax.psum_scatter(jnp.dot(dense_arrived, dense_joined, preferred_element_t...  24.5 us
    all_to_all x1, blocking collectives, on_device(): lax.all_to_all(normed, 'ep', split_axis=1, concat_axis=0, tiled=True)  16 us
  transfers between devices with their start and end apart: 8, of which 7 were waited for; matrix products, arithmetic and copies ran while one was open for 3% of the time, Pallas kernels for 0%

commit v1 on v0

--- a/solution.py
+++ b/solution.py
@@ -77,7 +77,7 @@
     )
     resid = (
         tokens.astype(jnp.float32)
-        + lax.psum(mixer_part.astype(jnp.bfloat16), "tp").astype(jnp.float32)
+        + jnp.sum(lax.all_gather(mixer_part.astype(jnp.bfloat16), "tp"), axis=0).astype(jnp.float32)
     ).astype(jnp.bfloat16)
     normed_ffn = rms_scale(resid, ffn_gain)
     router_logits = jnp.dot(normed_ffn, router_weight, preferred_element_type=jnp.float32)

time: 398 us -> 380 us (0.955)
  waiting for transfers between devices: 308 us -> 292 us
    psum x1 -> x0, waiting for transfers between devices: 41.6 us -> none  [on_device(): lax.psum(mixer_part.astype(jnp.bfloat16), 'tp').astype(jnp.float32)]
    all_gather x0 -> x1, waiting for transfers between devices: none -> 25.1 us  [on_device(): lax.all_gather(mixer_part.astype(jnp.bfloat16), 'tp')]
where the time goes in v1:
time: 380 us
  waiting for transfers between devices  292 us (77%)
  blocking collectives  30.1 us (8%)
  matrix products  26.9 us (7%)
  between operations  14.4 us (4%)
  starting transfers between devices  8.4 us (2%)
  other arithmetic  6.12 us (2%)
    all_gather x1, waiting for transfers between devices, on_device(): lax.all_gather(out_weight, 'ep', axis=1, tiled=True)  79.4 us
    psum x1, waiting for transfers between devices, on_device(): total = lax.psum(partial_value.astype(jnp.bfloat16), 'tp')  55.4 us
    all_gather x1, waiting for transfers between devices, on_device(): lax.all_gather(dense_down, 'ep', axis=1, tiled=True)  49.7 us
    reduce_scatter x1, waiting for transfers between devices, on_device(): lax.psum_scatter(jnp.dot(arrived, joined, preferred_element_type=jnp.floa...  30.9 us
    all_to_all x1, waiting for transfers between devices, on_device(): lax.all_to_all(total.reshape(sources, items, total.shape[1]), 'ep', split...  25.4 us
    all_gather x1, waiting for transfers between devices, on_device(): lax.all_gather(mixer_part.astype(jnp.bfloat16), 'tp')  25.1 us
    reduce_scatter x1, waiting for transfers between devices, on_device(): lax.psum_scatter(jnp.dot(dense_arrived, dense_joined, preferred_element_t...  24.5 us
    all_to_all x1, blocking collectives, on_device(): lax.all_to_all(normed, 'ep', split_axis=1, concat_axis=0, tiled=True)  16 us
  transfers between devices with their start and end apart: 8, of which 7 were waited for; matrix products, arithmetic and copies ran while one was open for 3% of the time, Pallas kernels for 0%

profile of v1, /device:TPU:0, one launch (start us, length us, event | category | flops | bytes accessed | tf_op | source)
XLA Modules:
  0.0 379.8 jit_solution(14939767746100767703)
XLA Ops:
  7.2 1.1 fusion.33
  8.4 1.1 fusion.35
  9.5 16.0 %all_to_all.48 = bf16[32,8,512]{2,0,1:T(8,128)(2,1)S(1)} all-to-all(bf16[32,8,512]{2,0,1:T(8,128)(2,1)S(1)} %bitcast.79), channel_id=1, replica_groups=mesh['ep'=8,'tp'=4] {'ep'}, dimensions={1} | all-to-all | bytes 524288 | tf_op jit(solution)/shard_map/all_to_all | solution.py:43
  25.5 3.4 convolution_convert_fusion.4
  29.7 30.9 %reduce-scatter.3.cloned.1.call-done = bf16[32,2048]{1,0:T(8,128)(2,1)} async-done(((bf16[256,2048]{1,0:T(8,128)(2,1)}), bf16[32,2048]{1,0:T(8,128)(2,1)}) %reduce-scatter.3.cloned.1.call-update) | async-done | bytes 131088 | tf_op jit(solution)/shard_map/reduce_scatter | solution.py:45
  60.7 0.9 slice_bitcast_fusion
  63.1 79.4 %all-gather.5.cloned.1.call-done = bf16[1024,4096]{1,0:T(8,128)(2,1)} async-done(((bf16[1024,512]{1,0:T(8,128)(2,1)}), bf16[1024,4096]{1,0:T(8,128)(2,1)}) %all-gather.5.cloned.1.call-update) | async-done | bytes 8388624 | tf_op jit(solution)/shard_map/all_gather | solution.py:75
  142.5 5.6 %convolution_convert_fusion.3 = bf16[32,4096]{1,0:T(8,128)(2,1)} fusion(bf16[1024,4096]{1,0:T(8,128)(2,1)} %all-gather.5.cloned.1.call-done, f32[32,1024]{1,0:T(8,128)S(1)} %multiply_add_fusion, bf16[32,2048]{1,0:T(8,128)(2,1)S(1)} %copy-done.4), kind=kOutput, calls=%fused_computation.6 | convolution fusion | flops 268926976 | bytes 8847360 | tf_op jit(solution)/shard_map/dot_general | solution.py:73
  148.2 25.1 %all-gather.9.cloned.1.call-done = bf16[128,4096]{1,0:T(8,128)(2,1)} async-done(((bf16[32,4096]{1,0:T(8,128)(2,1)}), bf16[128,4096]{1,0:T(8,128)(2,1)}) %all-gather.9.cloned.1.call-update) | async-done | bytes 1048592 | tf_op jit(solution)/shard_map/all_gather | solution.py:80
  173.3 1.4 reduce_sum.61
  175.1 14.1 %all_to_all.49 = bf16[32,8,512]{2,0,1:T(8,128)(2,1)S(1)} all-to-all(bf16[32,8,512]{2,0,1:T(8,128)(2,1)S(1)} %bitcast.80), channel_id=1, replica_groups=mesh['ep'=8,'tp'=4] {'ep'}, dimensions={1} | all-to-all | bytes 524288 | tf_op jit(solution)/shard_map/all_to_all | solution.py:132
  189.2 1.3 convolution_convert_fusion.5
  191.9 1.4 convolution_convert_fusion.1
  193.3 3.6 all-to-all-start.1
  196.9 24.5 %reduce-scatter.5.cloned.1.call-done = bf16[32,1024]{1,0:T(8,128)(2,1)} async-done(((bf16[256,1024]{1,0:T(8,128)(2,1)}), bf16[32,1024]{1,0:T(8,128)(2,1)}) %reduce-scatter.5.cloned.1.call-update) | async-done | bytes 65552 | tf_op jit(solution)/shard_map/reduce_scatter | solution.py:134
  221.3 0.8 convert_element_type.111
  222.2 49.7 %all-gather.7.cloned.1.call-done = bf16[512,4096]{1,0:T(8,128)(2,1)} async-done(((bf16[512,512]{1,0:T(8,128)(2,1)}), bf16[512,4096]{1,0:T(8,128)(2,1)}) %all-gather.7.cloned.1.call-update) | async-done | bytes 4194320 | tf_op jit(solution)/shard_map/all_gather | solution.py:147
  271.9 3.7 convolution_convert_fusion.2
  275.6 2.9 fusion.5
  278.6 5.9 %convolution_convert_fusion = bf16[128,4096]{1,0:T(8,128)(2,1)} fusion(bf16[1,512,4096]{2,1,0:T(8,128)(2,1)} %param.37, bf16[128,4096]{1,0:T(8,128)(2,1)S(1)} %bitcast.73, bf16[1,4096,512]{2,1,0:T(8,128)(2,1)} %param.36, f32[128,512]{1,0:T(8,128)S(1)} %fusion.5), kind=kOutput, calls=%fused_computation | convolution fusion | flops 1074659328 | bytes 10747904 | tf_op jit(solution)/shard_map/dot_general | solution.py:122
  284.5 55.4 %all-reduce.3.cloned.1.call-done = (bf16[8,16,4096]{2,1,0:T(8,128)(2,1)}, bf16[32,4096]{1,0:T(8,128)(2,1)}) async-done(((bf16[8,16,4096]{2,1,0:T(8,128)(2,1)}, bf16[32,4096]{1,0:T(8,128)(2,1)}), (bf16[8,16,4096]{2,1,0:T(8,128)(2,1)}, bf16[32,4096]{1,0:T(8,128)(2,1)})) %all-reduce.3.cloned.1.call-update) | async-done | bytes 1310736 | tf_op jit(solution)/shard_map/psum | solution.py:123
  339.8 4.6 %all-to-all-start.2 = ((bf16[8,16,4096]{2,1,0:T(8,128)(2,1)}), bf16[8,16,4096]{2,1,0:T(8,128)(2,1)S(1)}, u32[]{:S(2)}, u32[]{:S(2)}) async-start(bf16[8,16,4096]{2,1,0:T(8,128)(2,1)} %get-tuple-element.3), calls=%async_computation.3 | async-start | bytes 2097152 | tf_op jit(solution)/shard_map/all_to_all | solution.py:124
  345.6 25.4 %all-to-all-done.2 = bf16[8,16,4096]{2,1,0:T(8,128)(2,1)S(1)} async-done(((bf16[8,16,4096]{2,1,0:T(8,128)(2,1)}), bf16[8,16,4096]{2,1,0:T(8,128)(2,1)S(1)}, u32[]{:S(2)}, u32[]{:S(2)}) %all-to-all-start.2) | async-done | bytes 1048608 | tf_op jit(solution)/shard_map/all_to_all | solution.py:124
  371.0 2.0 fusion.1
  (76 shorter events, 5.2 us)
Async XLA Ops:
  7.2 54.7 %copy-start = (bf16[16,64,64]{2,1,0:T(8,128)(2,1)S(1)}, bf16[16,64,64]{2,1,0:T(8,128)(2,1)}, u32[]{:S(2)}) copy-start(bf16[16,64,64]{2,1,0:T(8,128)(2,1)} %param.28) | copy-start | bytes 393220
  7.2 53.5 %reduce-scatter.3.cloned.1.call-start = ((), (), s32[]{:S(2)}) async-start(), calls=%async_computation.6 | async-start | bytes 1179648 | tf_op jit(solution)/shard_map/reduce_scatter | solution.py:45
  8.4 21.3 %copy-start.11 = (f32[1024]{0:T(1024)S(1)}, f32[1024]{0:T(1024)}, u32[]{:S(2)}) copy-start(f32[1024]{0:T(1024)} %param.30) | copy-start | bytes 12292
  9.5 52.1 %copy-start.3 = (bf16[32,3,1024]{2,0,1:T(8,128)(2,1)S(1)}, bf16[32,3,1024]{2,0,1:T(8,128)(2,1)}, u32[]{:S(2)}) copy-start(bf16[32,3,1024]{2,0,1:T(8,128)(2,1)} %param.23) | copy-start | bytes 589828
  9.5 52.1 %copy-start.8 = (f32[4,1024]{1,0:T(4,128)S(1)}, f32[4,1024]{1,0:T(4,128)}, u32[]{:S(2)}) copy-start(f32[4,1024]{1,0:T(4,128)} %param.27) | copy-start | bytes 49156
  25.5 36.8 %copy-start.14 = (bf16[16,64,64]{2,1,0:T(8,128)(2,1)S(1)}, bf16[16,64,64]{2,1,0:T(8,128)(2,1)}, u32[]{:S(2)}) copy-start(bf16[16,64,64]{2,1,0:T(8,128)(2,1)} %param.29) | copy-start | bytes 393220
  28.9 34.0 %copy-start.5 = (f32[32,1024]{1,0:T(8,128)S(1)}, f32[32,1024]{1,0:T(8,128)}, u32[]{:S(2)}) copy-start(f32[32,1024]{1,0:T(8,128)} %param.22) | copy-start | bytes 393220
  28.9 113.6 %all-gather.5.cloned.1.call-start = ((), (), s32[]{:S(2)}) async-start(), calls=%async_computation.7 | async-start | bytes 9437184 | tf_op jit(solution)/shard_map/all_gather | solution.py:75
  29.7 143.6 %all-gather.9.cloned.1.call-start = ((), (), s32[]{:S(2)}) async-start(), calls=%async_computation.10 | async-start | bytes 1310720 | tf_op jit(solution)/shard_map/all_gather | solution.py:80
  60.7 81.8 %copy-start.4 = (bf16[32,2048]{1,0:T(8,128)(2,1)S(1)}, bf16[32,2048]{1,0:T(8,128)(2,1)}, u32[]{:S(2)}) copy-start(bf16[32,2048]{1,0:T(8,128)(2,1)} %reduce-scatter.3.cloned.1.call-done) | copy-start | bytes 393220
  63.0 85.1 %copy-start.2 = (f32[32,1024]{1,0:T(8,128)}, f32[32,1024]{1,0:T(8,128)S(1)}, u32[]{:S(2)}) copy-start(f32[32,1024]{1,0:T(8,128)S(1)} %multiply_add_fusion) | copy-start | bytes 393220
  63.0 111.7 %copy-start.1 = (bf16[32,4096]{1,0:T(8,128)(2,1)S(1)}, bf16[32,4096]{1,0:T(8,128)(2,1)}, u32[]{:S(2)}) copy-start(bf16[32,4096]{1,0:T(8,128)(2,1)} %param.21) | copy-start | bytes 786436
  63.0 111.9 %copy-start.7 = (f32[4096]{0:T(1024)S(1)}, f32[4096]{0:T(1024)}, u32[]{:S(2)}) copy-start(f32[4096]{0:T(1024)} %param.32) | copy-start | bytes 49156
  63.0 126.2 %copy-start.12 = (bf16[512,512]{1,0:T(8,128)(2,1)S(1)}, bf16[512,512]{1,0:T(8,128)(2,1)}, u32[]{:S(2)}) copy-start(bf16[512,512]{1,0:T(8,128)(2,1)} %param.39) | copy-start | bytes 1572868
  63.0 126.2 %copy-start.13 = (bf16[512,512]{1,0:T(8,128)(2,1)S(1)}, bf16[512,512]{1,0:T(8,128)(2,1)}, u32[]{:S(2)}) copy-start(bf16[512,512]{1,0:T(8,128)(2,1)} %param.38) | copy-start | bytes 1572868
  148.1 43.0 %copy-start.9 = (s32[32,2]{0,1:T(2,128)S(1)}, s32[32,2]{0,1:T(2,128)}, u32[]{:S(2)}) copy-start(s32[32,2]{0,1:T(2,128)} %param.34) | copy-start | bytes 772
  148.2 73.2 %reduce-scatter.5.cloned.1.call-start = ((), (), s32[]{:S(2)}) async-start(), calls=%async_computation.8 | async-start | bytes 589824 | tf_op jit(solution)/shard_map/reduce_scatter | solution.py:134
  190.5 81.4 %all-gather.7.cloned.1.call-start = ((), (), s32[]{:S(2)}) async-start(), calls=%async_computation.9 | async-start | bytes 4718592 | tf_op jit(solution)/shard_map/all_gather | solution.py:147
  193.3 82.4 %all-to-all-start.1 = ((bf16[8,16,4096]{2,1,0:T(8,128)(2,1)}), bf16[8,16,4096]{2,1,0:T(8,128)(2,1)S(1)}, u32[]{:S(2)}, u32[]{:S(2)}) async-start(bf16[8,16,4096]{2,1,0:T(8,128)(2,1)} %bitcast.10), calls=%async_computation.2 | async-start | bytes 2097152 | tf_op jit(solution)/shard_map/all_to_all | solution.py:116
  196.8 143.0 %all-reduce.3.cloned.1.call-start = ((), (), s32[]{:S(2)}) async-start(), calls=%async_computation.11 | async-start | bytes 2621440 | tf_op jit(solution)/shard_map/psum | solution.py:123
  278.5 65.9 %copy-start.10 = (bf16[4096]{0:T(1024)(128)(2,1)S(1)}, bf16[4096]{0:T(1024)(128)(2,1)}, u32[]{:S(2)}) copy-start(bf16[4096]{0:T(1024)(128)(2,1)} %param.41) | copy-start | bytes 24580
  278.6 66.6 %copy-start.6 = (bf16[4096,8]{0,1:T(8,128)(2,1)S(1)}, bf16[4096,8]{0,1:T(8,128)(2,1)}, u32[]{:S(2)}) copy-start(bf16[4096,8]{0,1:T(8,128)(2,1)} %param.33) | copy-start | bytes 196612
  339.8 31.2 %all-to-all-start.2 = ((bf16[8,16,4096]{2,1,0:T(8,128)(2,1)}), bf16[8,16,4096]{2,1,0:T(8,128)(2,1)S(1)}, u32[]{:S(2)}, u32[]{:S(2)}) async-start(bf16[8,16,4096]{2,1,0:T(8,128)(2,1)} %get-tuple-element.3), calls=%async_computation.3 | async-start | bytes 2097152 | tf_op jit(solution)/shard_map/all_to_all | solution.py:124
Sparse Core Ops, SparseCore 0:
  29.0 31.6 reduce-scatter.2
  62.3 80.1 all-gather.4
  148.3 24.9 all-gather.8
  190.6 30.6 reduce-scatter.4
  222.8 49.0 all-gather.6
  284.6 55.1 all-reduce.2
